TPU v7x, 32 devices: a whole 2x2x4 slice. The times are simulated.
32 devices in a mesh: sp: 8 (over z, x), tp: 4 (over y, core).
Axes of the slice: x: 2, y: 2, z: 4, core: 2. Of those that a mesh axis runs over, the one named last changes fastest.
Arguments:
- wide_query: bfloat16 [4096, 1536], P('sp', 'tp'), may hold values from -6 to 6
- wide_key: bfloat16 [4096, 1536], P('sp', 'tp'), may hold values from -6 to 6
- wide_value: bfloat16 [4096, 1536], P('sp', 'tp'), may hold values from -6 to 6
- wide_gate: bfloat16 [4096, 1536], P('sp', 'tp'), may hold values from -6 to 6
- narrow_query: bfloat16 [4096, 512], P('sp', 'tp'), may hold values from -6 to 6
- narrow_key: bfloat16 [4096, 512], P('sp', 'tp'), may hold values from -6 to 6
- narrow_value: bfloat16 [4096, 512], P('sp', 'tp'), may hold values from -6 to 6
- narrow_gate: bfloat16 [4096, 512], P('sp', 'tp'), may hold values from -6 to 6
- wide_decay: float32 [12, 4096], P('tp', 'sp'), may hold values from -1 to 0
- narrow_decay: float32 [8, 4096], P('tp', 'sp'), may hold values from -1 to 0
- residual: bfloat16 [4096, 2048], P(('sp', 'tp')), may hold values from -6 to 6
- wide_out: bfloat16 [1536, 2048], P('tp'), may hold values from -0.125 to 0.125
- narrow_out: bfloat16 [512, 2048], P('tp'), may hold values from -0.125 to 0.125
- up_weight: bfloat16 [2048, 8192], P('sp', 'tp'), may hold values from -0.125 to 0.125
- down_weight: bfloat16 [8192, 2048], P('tp', 'sp'), may hold values from -0.0625 to 0.0625
- gain_mix: float32 [2048], replicated, may hold values from 0.1 to 1.9
- gain_pre: float32 [2048], replicated, may hold values from 0.1 to 1.9
- gain_mlp: float32 [2048], replicated, may hold values from 0.1 to 1.9
Outputs:
- result: bfloat16 [4096, 2048], P(('sp', 'tp'))
All inputs are finite; a program needn't handle non-finite values.
Results may differ from a plain program's by a relative error of at most 0.02.
Values may be sent and summed in bfloat16 or wider, within the bound.
A program may use at most 128 MiB of HBM per device.

v0:
```python
import jax
import jax.numpy as jnp
from jax import lax
from jax.sharding import PartitionSpec as P

WIDE_DIM = 128
NARROW_DIM = 64
SPAN = 128
epsilon = 1e-06


def prefix_2(array, axis, join, neutral):
    place = lax.axis_index(axis)
    gathered = jax.tree.map(
        lambda a, kind: lax.all_gather(a.astype(kind), axis),
        array,
        (jnp.bfloat16, jnp.bfloat16, jnp.bfloat16, jnp.bfloat16),
    )
    state = jax.tree.map(lambda a, e: jnp.zeros_like(a) + jnp.asarray(e, a.dtype), array, neutral)

    def one(turn, state):
        return join(
            state,
            jax.tree.map(
                lambda a, own: lax.dynamic_index_in_dim(a, turn, 0, False).astype(own.dtype),
                gathered,
                array,
            ),
        )

    return lax.fori_loop(0, place, one, state)


def rotate(packed, head_dim, positions):
    length = packed.shape[0]
    grouped = packed.astype(jnp.float32).reshape(length, -1, head_dim)
    halfway = head_dim // 2
    inverse = 10000.0 ** (-jnp.arange(0, head_dim, 2, dtype=jnp.float32) / head_dim)
    angles = positions.astype(jnp.float32)[:, None] * inverse[None, :]
    cosine_table = jnp.cos(angles)[:, None, :]
    sine_table = jnp.sin(angles)[:, None, :]
    leading = grouped[..., :halfway]
    trailing = grouped[..., halfway:]
    return jnp.concatenate(
        [
            leading * cosine_table - trailing * sine_table,
            leading * sine_table + trailing * cosine_table,
        ],
        axis=-1,
    )


def rms_scale(values, gain_vector):
    return (
        values
        * lax.rsqrt(jnp.mean(values * values, axis=-1, keepdims=True) + epsilon)
        * gain_vector
    )


def span_terms(query, key, value, log_decay, head_dim, offset):
    length = query.shape[0]
    count_of_heads = query.shape[1] // head_dim
    span_count = length // SPAN
    shaped = (span_count, SPAN, count_of_heads, head_dim)
    positions = offset + jnp.arange(length, dtype=jnp.int32)
    queries = rotate(query, head_dim, positions).astype(jnp.bfloat16).reshape(shaped)
    keys_full = (rotate(key, head_dim, positions) * head_dim ** (-0.5)).reshape(shaped)
    keys_half = keys_full.astype(jnp.bfloat16)
    values_all = value.reshape(shaped)
    cumulative = jnp.cumsum(log_decay.T.reshape(span_count, SPAN, count_of_heads), axis=1)
    causal = jnp.arange(SPAN)[:, None] >= jnp.arange(SPAN)[None, :]
    scores = jnp.einsum("nihd,njhd->nhij", queries, keys_half, preferred_element_type=jnp.float32)
    decay_rows = cumulative.transpose(0, 2, 1)
    log_gaps = jnp.where(causal, decay_rows[..., :, None] - decay_rows[..., None, :], -jnp.inf)
    weights = (scores * jnp.exp(log_gaps)).astype(jnp.bfloat16)
    within = jnp.einsum("nhij,njhd->nihd", weights, values_all, preferred_element_type=jnp.float32)
    span_total = cumulative[:, -1, :]
    scaled = (keys_full * jnp.exp(span_total[:, None, :] - cumulative)[..., None]).astype(
        jnp.bfloat16
    )
    own_state = jnp.einsum(
        "njhd,njhe->nhde", scaled, values_all, preferred_element_type=jnp.float32
    )

    def advance(carried, inputs):
        decay_sum, contribution = inputs
        return (carried * jnp.exp(decay_sum)[:, None, None] + contribution, carried)

    initial = jnp.zeros((count_of_heads, head_dim, head_dim), jnp.float32)
    closing, before = lax.scan(advance, initial, (span_total, own_state))
    device_decay = jnp.exp(jnp.sum(span_total, axis=0))
    return (queries, cumulative, within, span_total, before, closing, device_decay)


def finish(parts, prefix, gate, head_dim):
    queries, cumulative, within, span_total, before, closing, device_decay = parts
    length = gate.shape[0]
    earlier = jnp.cumsum(span_total, axis=0) - span_total
    entering = (prefix[None] * jnp.exp(earlier)[:, :, None, None] + before).astype(jnp.bfloat16)
    across = (
        jnp.einsum("nihd,nhde->nihe", queries, entering, preferred_element_type=jnp.float32)
        * jnp.exp(cumulative)[..., None]
    )
    output = (within + across).reshape(length, -1, head_dim)
    normed = output * lax.rsqrt(jnp.mean(output * output, axis=-1, keepdims=True) + epsilon)
    return (normed.reshape(length, -1) * jax.nn.silu(gate.astype(jnp.float32))).astype(jnp.bfloat16)


def combine_states(former, latter):
    return (
        former[0] * latter[0],
        former[1] * latter[0][:, None, None] + latter[1],
        former[2] * latter[2],
        former[3] * latter[2][:, None, None] + latter[3],
    )


def local(
    wide_query,
    wide_key,
    wide_value,
    wide_gate,
    narrow_query,
    narrow_key,
    narrow_value,
    narrow_gate,
    wide_decay,
    narrow_decay,
    residual,
    wide_out,
    narrow_out,
    up_weight,
    down_weight,
    gain_mix,
    gain_pre,
    gain_mlp,
):
    length = wide_query.shape[0]
    offset = lax.axis_index("sp") * length
    wide_parts = span_terms(wide_query, wide_key, wide_value, wide_decay, WIDE_DIM, offset)
    narrow_parts = span_terms(
        narrow_query, narrow_key, narrow_value, narrow_decay, NARROW_DIM, offset
    )
    identity = (
        jnp.ones_like(wide_parts[6]),
        jnp.zeros_like(wide_parts[5]),
        jnp.ones_like(narrow_parts[6]),
        jnp.zeros_like(narrow_parts[5]),
    )
    prefixes = prefix_2(
        (wide_parts[6], wide_parts[5], narrow_parts[6], narrow_parts[5]),
        "sp",
        combine_states,
        identity,
    )
    wide_mixed = finish(wide_parts, prefixes[1], wide_gate, WIDE_DIM)
    narrow_mixed = finish(narrow_parts, prefixes[3], narrow_gate, NARROW_DIM)
    wide_rows, narrow_rows = (
        lax.all_to_all(wide_mixed, "tp", split_axis=0, concat_axis=1, tiled=True),
        lax.all_to_all(narrow_mixed, "tp", split_axis=0, concat_axis=1, tiled=True),
    )
    wide_whole, narrow_whole = (
        lax.all_gather(wide_out, "tp", axis=0, tiled=True),
        lax.all_gather(narrow_out, "tp", axis=0, tiled=True),
    )
    projected = jnp.dot(wide_rows, wide_whole, preferred_element_type=jnp.float32) + jnp.dot(
        narrow_rows, narrow_whole, preferred_element_type=jnp.float32
    )
    updated = (residual.astype(jnp.float32) + rms_scale(projected, gain_mix)).astype(jnp.bfloat16)
    normed = rms_scale(updated.astype(jnp.float32), gain_pre).astype(jnp.bfloat16)
    block_rows = lax.all_gather(normed, "tp", axis=0, tiled=True)
    rectified = jax.nn.relu(
        jnp.dot(
            block_rows,
            lax.all_gather(up_weight, "sp", axis=0, tiled=True),
            preferred_element_type=jnp.float32,
        )
    )
    hidden = (rectified * rectified).astype(jnp.bfloat16)
    partial_terms = jnp.dot(
        hidden,
        lax.all_gather(down_weight, "sp", axis=1, tiled=True),
        preferred_element_type=jnp.float32,
    )
    lowered = lax.psum_scatter(
        partial_terms.astype(jnp.bfloat16), "tp", scatter_dimension=0, tiled=True
    ).astype(jnp.float32)
    return (updated.astype(jnp.float32) + rms_scale(lowered, gain_mlp)).astype(jnp.bfloat16)


def solution(mesh):
    return jax.shard_map(
        local,
        mesh=mesh,
        in_specs=(
            P("sp", "tp"),
            P("sp", "tp"),
            P("sp", "tp"),
            P("sp", "tp"),
            P("sp", "tp"),
            P("sp", "tp"),
            P("sp", "tp"),
            P("sp", "tp"),
            P("tp", "sp"),
            P("tp", "sp"),
            P(("sp", "tp"), None),
            P("tp", None),
            P("tp", None),
            P("sp", "tp"),
            P("tp", "sp"),
            P(),
            P(),
            P(),
        ),
        out_specs=P(("sp", "tp"), None),
        check_vma=False,
    )
```

profile of v0, /device:TPU:0, one launch (start us, length us, event | category | flops | bytes accessed | tf_op | source)
XLA Modules:
  0.0 507.7 jit_solution(15633803309684791243)
XLA Ops:
  6.5 0.7 all-gather.10.cloned.1.call-update
  7.3 0.7 all-gather.12.cloned.1.call-update
  8.1 1.2 copy.77
  10.2 1.0 subtract_convert_fusion
  12.6 0.8 fusion.76
  13.6 0.8 fusion.33
  14.4 3.3 while.42
  14.4 0.7 bitcast_dynamic-update-slice_fusion.8
  15.2 0.7 bitcast_dynamic-update-slice_fusion.8
  16.0 0.7 bitcast_dynamic-update-slice_fusion.8
  16.9 0.7 bitcast_dynamic-update-slice_fusion.8
  17.7 33.8 %all-gather.1 = bf16[24,128,128]{2,1,0:T(8,128)(2,1)S(1)} all-gather(bf16[3,128,128]{2,1,0:T(8,128)(2,1)S(1)} %convert_element_type.154), channel_id=3, replica_groups=mesh['sp'=8,'tp'=4] {'sp'}, dimensions={0}, use_global_device_ids=true | all-gather | bytes 884736 | tf_op jit(solution)/shard_map/all_gather | solution.py:15
  51.6 1.0 multiply_cosine_fusion.1
  52.5 1.7 copy.93
  54.2 0.9 convert.30
  55.1 1.7 copy.106
  56.8 0.9 convert.31
  57.8 1.6 fusion.61
  59.4 0.7 bitcast_dynamic-update-slice_fusion.3
  60.1 0.9 copy.122
  61.0 1.2 reduce_window_sum.45
  62.2 0.6 fusion.75
  63.0 0.9 fusion.74
  63.9 1.1 copy.97
  65.0 1.8 reshape.384
  66.7 1.7 copy.99
  68.5 1.6 bitcast_dynamic-update-slice_fusion.2
  70.0 1.9 fusion.54
  71.9 6.2 %while.43 = (s32[]{:T(128)}, f32[2,64,64]{2,1,0:T(8,128)S(1)}, f32[4,2,64,64]{3,2,1,0:T(8,128)}, f32[4,2]{1,0:T(4,128)S(1)}, f32[4,2,64,64]{3,2,1,0:T(8,128)}, /*index=5*/s32[]{:T(128)}, s32[]{:T(128)}) while((s32[]{:T(128)}, f32[2,64,64]{2,1,0:T(8,128)S(1)}, f32[4,2,64,64]{3,2,1,0:T(8,128)}, f32[4,2]{1,0:T(4,128)S(1)}, ...), condition=%wide.region_7.8_spmd.clone, body=%wide.region_6.7_spmd.clone.sunk | while | flops 32771 | bytes 197240 | solution.py:91
  71.9 0.6 bitcast_dynamic-update-slice_fusion.9
  72.5 0.9 bitcast_add_fusion.5
  73.5 0.6 bitcast_dynamic-update-slice_fusion.9
  74.1 0.9 bitcast_add_fusion.5
  75.0 0.6 bitcast_dynamic-update-slice_fusion.9
  75.7 0.9 bitcast_add_fusion.5
  76.6 0.6 bitcast_dynamic-update-slice_fusion.9
  77.2 0.9 bitcast_add_fusion.5
  78.1 32.7 %all-gather.3 = bf16[16,64,64]{2,1,0:T(8,128)(2,1)} all-gather(bf16[2,64,64]{2,1,0:T(8,128)(2,1)S(1)} %convert_element_type.158), channel_id=5, replica_groups=mesh['sp'=8,'tp'=4] {'sp'}, dimensions={0}, use_global_device_ids=true | all-gather | bytes 147456 | tf_op jit(solution)/shard_map/all_gather | solution.py:15
  110.9 0.7 exponential_convert_fusion
  111.6 1.3 dynamic-slice
  114.6 21.4 %all-reduce.2 = (bf16[24]{0:T(256)(128)(2,1)S(1)}, bf16[16]{0:T(256)(128)(2,1)S(1)}) all-reduce(bf16[24]{0:T(256)(128)(2,1)S(1)} %dynamic-update-slice, bf16[16]{0:T(256)(128)(2,1)S(1)} %dynamic-update-slice.1), channel_id=2, replica_groups=mesh['sp'=8,'tp'=4] {'sp'}, use_global_device_ids=true, to_apply=%add | all-reduce | flops 40 | bytes 160
  136.2 1.0 concatenate.34
  137.5 1.7 concatenate.35
  139.1 1.2 copy.79
  140.3 1.1 copy.102
  142.1 2.6 fusion.8
  144.7 3.1 multiply_reduce_fusion.1
  147.8 1.7 copy.103
  149.6 1.2 copy.104
  151.0 0.8 copy_bitcast_fusion
  151.8 3.5 all-to-all-start
  157.2 0.7 copy_bitcast_fusion.1
  157.8 4.8 all-to-all-done
  162.7 3.3 all-to-all-start.1
  166.3 3.8 fusion.77
  170.6 2.1 multiply_reduce_fusion
  173.1 1.0 fusion.20
  175.4 24.6 %all-gather.14.cloned.1.call-done = bf16[512,2048]{1,0:T(8,128)(2,1)} async-done(((bf16[128,2048]{1,0:T(8,128)(2,1)}), bf16[512,2048]{1,0:T(8,128)(2,1)}) %all-gather.14.cloned.1.call-update) | async-done | bytes 2097168 | tf_op jit(solution)/shard_map/all_gather | solution.py:172
  200.0 126.5 %all-gather.16.cloned.1.call-done = bf16[2048,2048]{1,0:T(8,128)(2,1)} async-done(((bf16[256,2048]{1,0:T(8,128)(2,1)}), bf16[2048,2048]{1,0:T(8,128)(2,1)}) %all-gather.16.cloned.1.call-update) | async-done | bytes 8388624 | tf_op jit(solution)/shard_map/all_gather | solution.py:176
  326.4 125.0 %all-gather.18.cloned.1.call-done = bf16[2048,2048]{1,0:T(8,128)(2,1)} async-done(((bf16[2048,256]{1,0:T(8,128)(2,1)}), bf16[2048,2048]{1,0:T(8,128)(2,1)}) %all-gather.18.cloned.1.call-update) | async-done | bytes 8388624 | tf_op jit(solution)/shard_map/all_gather | solution.py:183
  451.5 16.5 %convolution_convert_fusion = bf16[512,2048]{1,0:T(8,128)(2,1)} fusion(bf16[2048,2048]{1,0:T(8,128)(2,1)} %all-gather.18.cloned.1.call-done, bf16[512,2048]{1,0:T(8,128)(2,1)} %all-gather.14.cloned.1.call-done, bf16[2048,2048]{1,0:T(8,128)(2,1)} %all-gather.16.cloned.1.call-done), kind=kOutput, calls=%fused_computation.19 | convolution fusion | flops 8594128896 | bytes 20971520 | tf_op jit(solution)/shard_map/dot_general | solution.py:181
  468.0 29.5 %reduce-scatter.2.cloned.1.call-done = bf16[128,2048]{1,0:T(8,128)(2,1)} async-done(((bf16[512,2048]{1,0:T(8,128)(2,1)}), bf16[128,2048]{1,0:T(8,128)(2,1)}) %reduce-scatter.2.cloned.1.call-update) | async-done | bytes 524304 | tf_op jit(solution)/shard_map/reduce_scatter | solution.py:186
  497.5 1.2 fusion.16
  498.8 2.1 fusion.21
  (121 shorter events, 9.3 us)
Async XLA Ops:
  6.5 2.8 copy-start.7
  6.5 159.7 %all-gather.10.cloned.1.call-start = ((), (), s32[]{:S(2)}) async-start(), calls=%async_computation.3 | async-start | bytes 7864320 | tf_op jit(solution)/shard_map/all_gather | solution.py:164
  7.3 163.3 %all-gather.12.cloned.1.call-start = ((), (), s32[]{:S(2)}) async-start(), calls=%async_computation.4 | async-start | bytes 2621440 | tf_op jit(solution)/shard_map/all_gather | solution.py:165
  9.6 2.5 copy-start.17
  10.2 3.2 copy-start.6
  14.4 45.7 %copy-start.18 = (f32[2,512]{1,0:T(2,128)S(1)}, f32[2,512]{1,0:T(2,128)}, u32[]{:S(2)}) copy-start(f32[2,512]{1,0:T(2,128)} %param.33) | copy-start | bytes 12292
  62.2 74.0 %copy-start = (f32[4,128,2]{2,1,0:T(8,128)}, f32[4,128,2]{2,1,0:T(8,128)S(1)}, u32[]{:S(2)}) copy-start(f32[4,128,2]{2,1,0:T(8,128)S(1)} %reduce_window_sum.45) | copy-start | bytes 12292
  62.9 1.0 copy-start.12
  144.7 11.0 %copy-start.1 = (f32[4,128,2]{2,1,0:T(8,128)S(1)}, f32[4,128,2]{2,1,0:T(8,128)}, u32[]{:S(2)}) copy-start(f32[4,128,2]{2,1,0:T(8,128)} %copy-done) | copy-start | bytes 12292
  144.7 11.1 %copy-start.8 = (bf16[2,4,4,8,128]{4,3,2,1,0:T(8,128)(2,1)S(1)}, bf16[2,4,4,8,128]{4,3,2,1,0:T(8,128)(2,1)}, u32[]{:S(2)}) copy-start(bf16[2,4,4,8,128]{4,3,2,1,0:T(8,128)(2,1)} %get-tuple-element.233) | copy-start | bytes 196612
  147.8 7.5 %copy-start.13 = (f32[4,1,2]{0,2,1:T(2,128)S(1)}, f32[4,1,2]{0,2,1:T(2,128)}, u32[]{:S(2)}) copy-start(f32[4,1,2]{0,2,1:T(2,128)} %copy-done.12) | copy-start | bytes 100
  147.8 7.7 %copy-start.2 = (f32[4,128,2]{2,1,0:T(8,128)S(1)}, f32[4,128,2]{2,1,0:T(8,128)}, u32[]{:S(2)}) copy-start(f32[4,128,2]{2,1,0:T(8,128)} %get-tuple-element.236) | copy-start | bytes 12292
  147.8 8.1 %copy-start.9 = (f32[4,2,64,64]{3,2,1,0:T(8,128)S(1)}, f32[4,2,64,64]{3,2,1,0:T(8,128)}, u32[]{:S(2)}) copy-start(f32[4,2,64,64]{3,2,1,0:T(8,128)} %get-tuple-element.136) | copy-start | bytes 393220
  147.8 8.4 %copy-start.3 = (f32[4,128,2,64]{1,3,2,0:T(8,128)S(1)}, f32[4,128,2,64]{1,3,2,0:T(8,128)}, u32[]{:S(2)}) copy-start(f32[4,128,2,64]{1,3,2,0:T(8,128)} %bitcast_dynamic-update-slice_fusion.2) | copy-start | bytes 786436
  147.8 8.4 %copy-start.4 = (bf16[4,128,2,64]{1,3,2,0:T(8,128)(2,1)S(1)}, bf16[4,128,2,64]{1,3,2,0:T(8,128)(2,1)}, u32[]{:S(2)}) copy-start(bf16[4,128,2,64]{1,3,2,0:T(8,128)(2,1)} %copy.99) | copy-start | bytes 393220
  147.8 8.4 %copy-start.11 = (pred[128,128]{1,0:T(8,128)(4,1)S(1)}, pred[128,128]{1,0:T(8,128)(4,1)}, u32[]{:S(2)}) copy-start(pred[128,128]{1,0:T(8,128)(4,1)} %iota_compare_fusion) | copy-start | bytes 49156
  147.8 9.1 %copy-start.10 = (bf16[512,128]{1,0:T(8,128)(2,1)S(1)}, bf16[512,128]{1,0:T(8,128)(2,1)}, u32[]{:S(2)}) copy-start(bf16[512,128]{1,0:T(8,128)(2,1)} %param.31) | copy-start | bytes 393220
  151.8 10.8 %all-to-all-start = ((bf16[4,128,384]{1,2,0:T(8,128)(2,1)}), bf16[4,128,384]{1,2,0:T(8,128)(2,1)S(1)}, u32[]{:S(2)}, u32[]{:S(2)}) async-start(bf16[4,128,384]{1,2,0:T(8,128)(2,1)} %copy_bitcast_fusion), calls=%async_computation | async-start | bytes 786432 | tf_op jit(solution)/shard_map/all_to_all | solution.py:160
  162.7 7.9 %all-to-all-start.1 = ((bf16[4,128,128]{1,2,0:T(8,128)(2,1)}), bf16[4,128,128]{1,2,0:T(8,128)(2,1)S(1)}, u32[]{:S(2)}, u32[]{:S(2)}) async-start(bf16[4,128,128]{1,2,0:T(8,128)(2,1)} %copy_bitcast_fusion.1), calls=%async_computation.1 | async-start | bytes 262144 | tf_op jit(solution)/shard_map/all_to_all | solution.py:161
  166.0 34.0 %all-gather.14.cloned.1.call-start = ((), (), s32[]{:S(2)}) async-start(), calls=%async_computation.5 | async-start | bytes 2621440 | tf_op jit(solution)/shard_map/all_gather | solution.py:172
  170.1 2.7 copy-start.5
  170.1 2.7 copy-start.14
  170.1 3.0 copy-start.15
  174.1 152.3 %all-gather.16.cloned.1.call-start = ((), (), s32[]{:S(2)}) async-start(), calls=%async_computation.6 | async-start | bytes 9437184 | tf_op jit(solution)/shard_map/all_gather | solution.py:176
  174.7 276.8 %all-gather.18.cloned.1.call-start = ((), (), s32[]{:S(2)}) async-start(), calls=%async_computation.7 | async-start | bytes 9437184 | tf_op jit(solution)/shard_map/all_gather | solution.py:183
  175.3 323.5 %copy-start.16 = (f32[2048]{0:T(1024)S(1)}, f32[2048]{0:T(1024)}, u32[]{:S(2)}) copy-start(f32[2048]{0:T(1024)} %param.41) | copy-start | bytes 24580
  175.3 322.2 %reduce-scatter.2.cloned.1.call-start = ((), (), s32[]{:S(2)}) async-start(), calls=%async_computation.8 | async-start | bytes 2621440 | tf_op jit(solution)/shard_map/reduce_scatter | solution.py:186
Sparse Core Ops, SparseCore 0:
  8.9 49.0 all-gather.9
  59.6 22.5 all-gather.11
  174.3 25.6 all-gather.13
  201.9 124.4 all-gather.15
  328.3 123.1 all-gather.17
  468.1 29.3 reduce-scatter.1
where the time goes:
time: 509 us; the launch traced here: 508 us
  waiting for transfers between devices  313 us (61%)
  blocking collectives  88 us (17%)
  matrix products  31.6 us (6%)
  local copies, waits for them, and re-layouts  26.2 us (5%)
  other arithmetic  26.1 us (5%)
  between operations  15.2 us (3%)
  starting transfers between devices  7.16 us (1%)
    all_gather x1, waiting for transfers between devices, local(): lax.all_gather(up_weight, 'sp', axis=0, tiled=True)  126 us
    all_gather x1, waiting for transfers between devices, local(): lax.all_gather(down_weight, 'sp', axis=1, tiled=True)  125 us
    all_gather x2, blocking collectives, prefix_2(): lax.all_gather(a.astype(kind), axis)  66.6 us
    reduce_scatter x1, waiting for transfers between devices, local(): lax.psum_scatter(partial_terms.astype(jnp.bfloat16), 'tp', scatter_dimens...  29.5 us
    all_gather x1, waiting for transfers between devices, local(): block_rows = lax.all_gather(normed, 'tp', axis=0, tiled=True)  24.6 us
    unnamed x1, blocking collectives  21.4 us
    dot_general x1, matrix products, local(): jnp.dot(hidden, lax.all_gather(down_weight, 'sp', axis=1, tiled=True), pr...  16.5 us
  transfers between devices with their start and end apart: 8, of which 6 were waited for; matrix products, arithmetic and copies ran while one was open for 12% of the time, Pallas kernels for 0%

commit v1 on v0

--- a/solution.py
+++ b/solution.py
@@ -180,7 +180,7 @@
     hidden = (rectified * rectified).astype(jnp.bfloat16)
     partial_terms = jnp.dot(
         hidden,
-        lax.all_gather(down_weight, "sp", axis=1, tiled=True),
+        jnp.concatenate(lax.all_gather(down_weight, "sp"), axis=1),
         preferred_element_type=jnp.float32,
     )
     lowered = lax.psum_scatter(

time: 509 us -> 422 us (0.83)
  waiting for transfers between devices: 313 us -> 220 us
  local copies, waits for them, and re-layouts: 26.2 us -> 33.1 us
  blocking collectives: 88 us -> 94.7 us
  other arithmetic: 26.1 us -> 20 us
    all_gather x1, waiting for transfers between devices: 125 us -> 45.1 us  [local(): lax.all_gather(down_weight, 'sp')]
    all_gather x1, waiting for transfers between devices: 24.6 us -> 10.6 us  [local(): block_rows = lax.all_gather(normed, 'tp', axis=0, tiled=True)]
    reshape x0 -> x1, local copies, waits for them, and re-layouts: none -> 11.6 us  [local(): jnp.concatenate(lax.all_gather(down_weight, 'sp'), axis=1)]
  transfers between devices with their start and end apart: 8 -> 8, of which waited for: 6 -> 6; matrix products, arithmetic and copies ran while one was open for 12% -> 15% of each run, Pallas kernels for 0% -> 0%
where the time goes in v1:
time: 422 us; the launch traced here: 420 us
  waiting for transfers between devices  220 us (52%)
  blocking collectives  94.7 us (22%)
  local copies, waits for them, and re-layouts  33.1 us (8%)
  matrix products  29.9 us (7%)
  other arithmetic  20 us (5%)
  between operations  15.4 us (4%)
  starting transfers between devices  7.16 us (2%)
    all_gather x1, waiting for transfers between devices, local(): lax.all_gather(up_weight, 'sp', axis=0, tiled=True)  126 us
    all_gather x2, blocking collectives, prefix_2(): lax.all_gather(a.astype(kind), axis)  71 us
    all_gather x1, waiting for transfers between devices, local(): lax.all_gather(down_weight, 'sp')  45.1 us
    reduce_scatter x1, waiting for transfers between devices, local(): lax.psum_scatter(partial_terms.astype(jnp.bfloat16), 'tp', scatter_dimens...  29.5 us
    unnamed x1, blocking collectives  23.7 us
    dot_general x1, matrix products, local(): jnp.dot(hidden, jnp.concatenate(lax.all_gather(down_weight, 'sp'), axis=1...  16.5 us
    reshape x1, local copies, waits for them, and re-layouts, local(): jnp.concatenate(lax.all_gather(down_weight, 'sp'), axis=1)  11.6 us
    all_gather x1, waiting for transfers between devices, local(): block_rows = lax.all_gather(normed, 'tp', axis=0, tiled=True)  10.6 us
  transfers between devices with their start and end apart: 8, of which 6 were waited for; matrix products, arithmetic and copies ran while one was open for 15% of the time, Pallas kernels for 0%

profile of v1, /device:TPU:0, one launch (start us, length us, event | category | flops | bytes accessed | tf_op | source)
XLA Modules:
  0.0 420.1 jit_solution(10806266527916559806)
XLA Ops:
  6.5 0.7 all-gather.11.cloned.1.call-update
  7.3 0.7 all-gather.13.cloned.1.call-update
  8.1 0.7 all-gather.19.cloned.1.call-update
  8.8 1.2 copy.119
  10.4 0.5 multiply_cosine_fusion
  11.0 1.0 subtract_convert_fusion
  13.8 0.6 dynamic-slice
  16.2 0.6 reduce_window_sum.46
  16.8 23.7 %all-reduce.2 = (bf16[24]{0:T(256)(128)(2,1)}, bf16[16]{0:T(256)(128)(2,1)}) all-reduce(bf16[24]{0:T(256)(128)(2,1)S(1)} %dynamic-update-slice, bf16[16]{0:T(256)(128)(2,1)S(1)} %dynamic-update-slice.1), channel_id=2, replica_groups=mesh['sp'=8,'tp'=4] {'sp'}, use_global_device_ids=true, to_apply=%add | all-reduce | flops 40 | bytes 160
  40.5 0.8 fusion.76
  41.3 1.4 reshape.394
  42.8 0.8 fusion.33
  43.6 3.3 while.42
  43.6 0.7 bitcast_dynamic-update-slice_fusion.8
  44.4 0.7 bitcast_dynamic-update-slice_fusion.8
  45.2 0.7 bitcast_dynamic-update-slice_fusion.8
  46.0 0.7 bitcast_dynamic-update-slice_fusion.8
  46.9 0.7 convert_element_type.154
  47.5 1.0 copy.135
  48.6 1.0 copy.148
  49.7 0.6 copy-done.14
  50.4 0.8 fusion.74
  51.9 0.7 fusion.61
  52.9 2.9 while.43
  52.9 0.6 bitcast_dynamic-update-slice_fusion.9
  53.6 0.6 bitcast_dynamic-update-slice_fusion.9
  54.4 0.6 bitcast_dynamic-update-slice_fusion.9
  55.1 0.6 bitcast_dynamic-update-slice_fusion.9
  55.8 0.6 convert_element_type.158
  56.4 1.3 reshape.378
  57.7 1.3 reshape.380
  59.0 1.0 concatenate.34
  60.3 0.7 concatenate.35
  61.0 1.2 copy.121
  62.2 1.1 copy.144
  63.3 1.1 copy.126
  64.4 33.3 %all-gather.3 = bf16[16,64,64]{2,1,0:T(8,128)(2,1)} all-gather(bf16[2,64,64]{2,1,0:T(8,128)(2,1)} %convert_element_type.158), channel_id=5, replica_groups=mesh['sp'=8,'tp'=4] {'sp'}, dimensions={0}, use_global_device_ids=true | all-gather | bytes 147456 | tf_op jit(solution)/shard_map/all_gather | solution.py:15
  97.7 0.6 iota_compare_fusion
  98.3 1.3 subtract_exponential_fusion
  99.6 37.7 %all-gather.1 = bf16[24,128,128]{2,1,0:T(8,128)(2,1)} all-gather(bf16[3,128,128]{2,1,0:T(8,128)(2,1)} %convert_element_type.154), channel_id=3, replica_groups=mesh['sp'=8,'tp'=4] {'sp'}, dimensions={0}, use_global_device_ids=true | all-gather | bytes 884736 | tf_op jit(solution)/shard_map/all_gather | solution.py:15
  137.3 2.6 fusion.8
  139.9 3.1 multiply_reduce_fusion.1
  143.1 1.8 copy.145
  144.9 1.2 copy.146
  146.3 0.8 copy_bitcast_fusion
  147.1 3.5 all-to-all-start
  151.6 0.5 multiply_reduce_fusion.2
  152.5 0.7 copy_bitcast_fusion.1
  153.1 4.8 %all-to-all-done = bf16[4,128,384]{1,2,0:T(8,128)(2,1)S(1)} async-done(((bf16[4,128,384]{1,2,0:T(8,128)(2,1)}), bf16[4,128,384]{1,2,0:T(8,128)(2,1)S(1)}, u32[]{:S(2)}, u32[]{:S(2)}) %all-to-all-start) | async-done | bytes 393248 | tf_op jit(solution)/shard_map/all_to_all | solution.py:160
  158.0 3.3 all-to-all-start.1
  161.6 3.8 fusion.77
  165.4 0.5 all-to-all-done.1
  165.9 2.1 multiply_reduce_fusion
  168.1 0.4 fusion.18
  168.5 1.0 fusion.20
  169.5 0.5 all-gather.17.cloned.1.call-update
  170.1 45.1 %all-gather.19.cloned.1.call-done = bf16[16384,256]{1,0:T(8,128)(2,1)} async-done(((bf16[2048,256]{1,0:T(8,128)(2,1)}), bf16[16384,256]{1,0:T(8,128)(2,1)}) %all-gather.19.cloned.1.call-update) | async-done | bytes 8388624 | tf_op jit(solution)/shard_map/all_gather | solution.py:183
  215.2 11.6 %copy.160 = bf16[2048,8,256]{0,2,1:T(8,128)(2,1)} copy(bf16[2048,8,256]{2,0,1:T(8,128)(2,1)} %bitcast.172) | data formatting | bytes 16777216 | tf_op jit(solution)/shard_map/reshape | solution.py:183
  226.7 10.6 %all-gather.15.cloned.1.call-done = bf16[512,2048]{1,0:T(8,128)(2,1)} async-done(((bf16[128,2048]{1,0:T(8,128)(2,1)}), bf16[512,2048]{1,0:T(8,128)(2,1)}) %all-gather.15.cloned.1.call-update) | async-done | bytes 2097168 | tf_op jit(solution)/shard_map/all_gather | solution.py:172
  237.4 126.5 %all-gather.17.cloned.1.call-done = bf16[2048,2048]{1,0:T(8,128)(2,1)} async-done(((bf16[256,2048]{1,0:T(8,128)(2,1)}), bf16[2048,2048]{1,0:T(8,128)(2,1)}) %all-gather.17.cloned.1.call-update) | async-done | bytes 8388624 | tf_op jit(solution)/shard_map/all_gather | solution.py:176
  363.8 16.5 %convolution_convert_fusion = bf16[512,2048]{1,0:T(8,128)(2,1)} fusion(bf16[2048,2048]{0,1:T(8,128)(2,1)} %bitcast.173, bf16[512,2048]{1,0:T(8,128)(2,1)} %all-gather.15.cloned.1.call-done, bf16[2048,2048]{1,0:T(8,128)(2,1)} %all-gather.17.cloned.1.call-done), kind=kOutput, calls=%fused_computation.19 | convolution fusion | flops 8594128896 | bytes 20971520 | tf_op jit(solution)/shard_map/dot_general | solution.py:181
  380.4 29.5 %reduce-scatter.2.cloned.1.call-done = bf16[128,2048]{1,0:T(8,128)(2,1)} async-done(((bf16[512,2048]{1,0:T(8,128)(2,1)}), bf16[128,2048]{1,0:T(8,128)(2,1)}) %reduce-scatter.2.cloned.1.call-update) | async-done | bytes 524304 | tf_op jit(solution)/shard_map/reduce_scatter | solution.py:186
  409.9 1.2 fusion.16
  411.1 2.1 fusion.21
  (128 shorter events, 7.0 us)
Async XLA Ops:
  6.5 3.6 copy-start.6
  6.5 155.0 %all-gather.11.cloned.1.call-start = ((), (), s32[]{:S(2)}) async-start(), calls=%async_computation.3 | async-start | bytes 7864320 | tf_op jit(solution)/shard_map/all_gather | solution.py:164
  7.3 158.6 %all-gather.13.cloned.1.call-start = ((), (), s32[]{:S(2)}) async-start(), calls=%async_computation.4 | async-start | bytes 2621440 | tf_op jit(solution)/shard_map/all_gather | solution.py:165
  8.0 207.2 %all-gather.19.cloned.1.call-start = ((), (), s32[]{:S(2)}) async-start(), calls=%async_computation.8 | async-start | bytes 9437184 | tf_op jit(solution)/shard_map/all_gather | solution.py:183
  10.3 2.6 copy-start.19
  10.4 2.9 copy-start.20
  10.9 2.8 copy-start.21
  13.3 28.0 %copy-start = (f32[4,128,3]{2,1,0:T(8,128)}, f32[4,128,3]{2,1,0:T(8,128)S(1)}, u32[]{:S(2)}) copy-start(f32[4,128,3]{2,1,0:T(8,128)S(1)} %reduce_window_sum.44) | copy-start | bytes 18436
  43.6 7.7 %copy-start.10 = (bf16[512,128]{1,0:T(8,128)(2,1)S(1)}, bf16[512,128]{1,0:T(8,128)(2,1)}, u32[]{:S(2)}) copy-start(bf16[512,128]{1,0:T(8,128)(2,1)} %param.30) | copy-start | bytes 393220
  46.8 13.4 %copy-start.13 = (f32[4,3]{1,0:T(4,128)}, f32[4,3]{1,0:T(4,128)S(1)}, u32[]{:S(2)}) copy-start(f32[4,3]{1,0:T(4,128)S(1)} %get-tuple-element.474) | copy-start | bytes 148
  47.5 12.8 %copy-start.2 = (bf16[512,3,64]{0,2,1:T(8,128)(2,1)S(1)}, bf16[512,3,64]{0,2,1:T(8,128)(2,1)}, u32[]{:S(2)}) copy-start(bf16[512,3,64]{0,2,1:T(8,128)(2,1)} %get-tuple-element.234) | copy-start | bytes 589828
  49.7 0.6 copy-start.14
  52.7 6.3 %copy-start.3 = (f32[4,128,2,64]{1,3,2,0:T(8,128)}, f32[4,128,2,64]{1,3,2,0:T(8,128)S(1)}, u32[]{:S(2)}) copy-start(f32[4,128,2,64]{1,3,2,0:T(8,128)S(1)} %bitcast_dynamic-update-slice_fusion.2) | copy-start | bytes 786436
  139.9 11.2 %copy-start.8 = (bf16[2,4,4,8,128]{4,3,2,1,0:T(8,128)(2,1)S(1)}, bf16[2,4,4,8,128]{4,3,2,1,0:T(8,128)(2,1)}, u32[]{:S(2)}) copy-start(bf16[2,4,4,8,128]{4,3,2,1,0:T(8,128)(2,1)} %get-tuple-element.238) | copy-start | bytes 196612
  143.0 7.6 %copy-start.15 = (f32[4,1,2]{0,2,1:T(2,128)S(1)}, f32[4,1,2]{0,2,1:T(2,128)}, u32[]{:S(2)}) copy-start(f32[4,1,2]{0,2,1:T(2,128)} %copy-done.14) | copy-start | bytes 100
  143.0 7.8 %copy-start.1 = (f32[4,128,2]{2,1,0:T(8,128)S(1)}, f32[4,128,2]{2,1,0:T(8,128)}, u32[]{:S(2)}) copy-start(f32[4,128,2]{2,1,0:T(8,128)} %get-tuple-element.241) | copy-start | bytes 12292
  143.0 8.1 %copy-start.7 = (bf16[2,4,4,8,128]{4,3,2,1,0:T(8,128)(2,1)S(1)}, bf16[2,4,4,8,128]{4,3,2,1,0:T(8,128)(2,1)}, u32[]{:S(2)}) copy-start(bf16[2,4,4,8,128]{4,3,2,1,0:T(8,128)(2,1)} %get-tuple-element.237) | copy-start | bytes 196612
  143.0 8.2 %copy-start.9 = (f32[4,2,64,64]{3,2,1,0:T(8,128)S(1)}, f32[4,2,64,64]{3,2,1,0:T(8,128)}, u32[]{:S(2)}) copy-start(f32[4,2,64,64]{3,2,1,0:T(8,128)} %get-tuple-element.136) | copy-start | bytes 393220
  143.0 8.5 %copy-start.4 = (f32[4,128,2,64]{1,3,2,0:T(8,128)S(1)}, f32[4,128,2,64]{1,3,2,0:T(8,128)}, u32[]{:S(2)}) copy-start(f32[4,128,2,64]{1,3,2,0:T(8,128)} %copy-done.3) | copy-start | bytes 786436
  143.1 8.5 %copy-start.12 = (pred[128,128]{1,0:T(8,128)(4,1)S(1)}, pred[128,128]{1,0:T(8,128)(4,1)}, u32[]{:S(2)}) copy-start(pred[128,128]{1,0:T(8,128)(4,1)} %iota_compare_fusion) | copy-start | bytes 49156
  143.1 9.2 %copy-start.11 = (bf16[512,128]{1,0:T(8,128)(2,1)S(1)}, bf16[512,128]{1,0:T(8,128)(2,1)}, u32[]{:S(2)}) copy-start(bf16[512,128]{1,0:T(8,128)(2,1)} %param.31) | copy-start | bytes 393220
  147.1 10.8 %all-to-all-start = ((bf16[4,128,384]{1,2,0:T(8,128)(2,1)}), bf16[4,128,384]{1,2,0:T(8,128)(2,1)S(1)}, u32[]{:S(2)}, u32[]{:S(2)}) async-start(bf16[4,128,384]{1,2,0:T(8,128)(2,1)} %copy_bitcast_fusion), calls=%async_computation | async-start | bytes 786432 | tf_op jit(solution)/shard_map/all_to_all | solution.py:160
  158.0 7.9 %all-to-all-start.1 = ((bf16[4,128,128]{1,2,0:T(8,128)(2,1)}), bf16[4,128,128]{1,2,0:T(8,128)(2,1)S(1)}, u32[]{:S(2)}, u32[]{:S(2)}) async-start(bf16[4,128,128]{1,2,0:T(8,128)(2,1)} %copy_bitcast_fusion.1), calls=%async_computation.1 | async-start | bytes 262144 | tf_op jit(solution)/shard_map/all_to_all | solution.py:161
  161.3 76.0 %all-gather.15.cloned.1.call-start = ((), (), s32[]{:S(2)}) async-start(), calls=%async_computation.5 | async-start | bytes 2621440 | tf_op jit(solution)/shard_map/all_gather | solution.py:172
  165.4 2.7 copy-start.5
  165.4 2.7 copy-start.16
  165.4 3.0 copy-start.17
  169.5 194.4 %all-gather.17.cloned.1.call-start = ((), (), s32[]{:S(2)}) async-start(), calls=%async_computation.6 | async-start | bytes 9437184 | tf_op jit(solution)/shard_map/all_gather | solution.py:176
  170.1 239.9 %reduce-scatter.2.cloned.1.call-start = ((), (), s32[]{:S(2)}) async-start(), calls=%async_computation.7 | async-start | bytes 2621440 | tf_op jit(solution)/shard_map/reduce_scatter | solution.py:186
  363.8 47.3 %copy-start.18 = (f32[2048]{0:T(1024)S(1)}, f32[2048]{0:T(1024)}, u32[]{:S(2)}) copy-start(f32[2048]{0:T(1024)} %param.41) | copy-start | bytes 24580
Sparse Core Ops, SparseCore 0:
  8.9 49.0 all-gather.10
  59.6 22.5 all-gather.12
  84.3 130.8 all-gather.18
  216.6 20.7 all-gather.14
  239.3 124.4 all-gather.16
  380.5 29.3 reduce-scatter.1
